TPU v7x, 32 devices: a whole 2x2x4 slice. The times are simulated.
32 devices in a mesh: sp: 16 (over z, y, x), tp: 2 (over core).
Axes of the slice: x: 2, y: 2, z: 4, core: 2. Of those that a mesh axis runs over, the one named last changes fastest.
Arguments:
- tokens: bfloat16 [4096, 2048], P('sp', 'tp'), may hold values from -24 to 24
- value_weight: bfloat16 [2, 2048, 2048], P(None, 'sp', 'tp'), may hold values from -0.125 to 0.125
- outer_weight: bfloat16 [2, 2048, 2048], P(None, 'sp', 'tp'), may hold values from -0.125 to 0.125
- inner_weight: bfloat16 [2, 2048, 2048], P(None, 'sp', 'tp'), may hold values from -0.125 to 0.125
- conv_taps: float32 [2, 3, 2048], P(None, None, 'tp'), may hold values from -3.5 to 3.5
- output_weight: bfloat16 [2, 2048, 2048], P(None, 'tp', 'sp'), may hold values from -2 to 2
- norm_gain: float32 [2, 2048], P(None, 'tp'), may hold values from 0.1 to 1.9
- norm_bias: float32 [2, 2048], P(None, 'tp'), may hold values from -3 to 3
Outputs:
- mixed_out: bfloat16 [4096, 2048], P('sp', 'tp')
All inputs are finite; a program needn't handle non-finite values.
Results may differ from a plain program's by a relative error of at most 0.03.
Values may be sent and summed in bfloat16 or wider, within the bound.
A program may use at most 64 MiB of HBM per device.

v0:
```python
import jax
import jax.numpy as jnp
from jax import lax
from jax.sharding import PartitionSpec as P

D = 2048
LAYERS = 2


def from_behind(array, axis, by):
    peers = lax.axis_size(axis)
    pairs = [(i, i + by) for i in range(peers) if 0 <= i + by < peers]
    return lax.ppermute(array, axis, pairs)


def input_products(whole, weights):
    return tuple(
        (
            jnp.dot(whole, weight, preferred_element_type=jnp.float32).astype(jnp.bfloat16)
            for weight in weights
        )
    )


def shards(
    tokens, value_weight, outer_weight, inner_weight, conv_taps, output_weight, norm_gain, norm_bias
):
    alpha = (2.0 * LAYERS) ** 0.25
    state = tokens
    taps_count = conv_taps.shape[1]
    all_value, all_outer, all_inner, all_output = (
        lax.all_gather(value_weight, "sp", axis=1, tiled=True),
        lax.all_gather(outer_weight, "sp", axis=1, tiled=True),
        lax.all_gather(inner_weight, "sp", axis=1, tiled=True),
        lax.all_gather(output_weight, "sp", axis=2, tiled=True),
    )
    for layer in range(LAYERS):
        whole = lax.all_gather(state, "tp", axis=1, tiled=True)
        u_part, outer, inner = input_products(
            whole, (all_value[layer], all_outer[layer], all_inner[layer])
        )
        gated_in = inner.astype(jnp.float32) * u_part.astype(jnp.float32)
        previous = from_behind(gated_in[gated_in.shape[0] - (taps_count - 1) :], "sp", 1)
        padded = jnp.concatenate([previous, gated_in], axis=0)
        conv = jnp.zeros_like(gated_in)
        for tap in range(taps_count):
            conv = conv + conv_taps[layer, tap][None, :] * padded[tap : tap + gated_in.shape[0]]
        gated = (outer.astype(jnp.float32) * conv).astype(jnp.bfloat16)
        terms = jnp.dot(gated, all_output[layer], preferred_element_type=jnp.float32)
        branch = lax.psum_scatter(
            terms.astype(jnp.bfloat16), "tp", scatter_dimension=1, tiled=True
        ).astype(jnp.float32)
        pre = alpha * state.astype(jnp.float32) + branch
        total, squares = lax.psum(
            (jnp.sum(pre, axis=-1, keepdims=True), jnp.sum(pre * pre, axis=-1, keepdims=True)), "tp"
        )
        mean = total / D
        var = jnp.maximum(squares / D - mean * mean, 0.0)
        normed = (pre - mean) * lax.rsqrt(var + 1e-05)
        state = (normed * norm_gain[layer][None, :] + norm_bias[layer][None, :]).astype(
            jnp.bfloat16
        )
    return state


def solution(mesh):
    in_specs = (
        P("sp", "tp"),
        P(None, "sp", "tp"),
        P(None, "sp", "tp"),
        P(None, "sp", "tp"),
        P(None, None, "tp"),
        P(None, "tp", "sp"),
        P(None, "tp"),
        P(None, "tp"),
    )
    out_specs = P("sp", "tp")
    return jax.shard_map(shards, mesh=mesh, in_specs=in_specs, out_specs=out_specs, check_vma=False)
```

profile of v0, /device:TPU:0, one launch (start us, length us, event | category | flops | bytes accessed | tf_op | source)
XLA Modules:
  0.0 578.4 jit_solution(5210033657117156722)
XLA Ops:
  6.5 0.7 all-gather.7.cloned.1.call-update
  7.3 0.7 all-gather.13.cloned.1.call-update
  8.0 0.0 all-gather.11.cloned.1.call-start
  8.1 0.7 all-gather.11.cloned.1.call-update
  8.8 0.5 all-gather.15.cloned.1.call-update
  9.4 0.5 all-gather.9.cloned.1.call-update
  9.9 0.0 reduce-scatter.3.cloned.1.call-start
  10.0 10.7 %all-gather.7.cloned.1.call-done = bf16[256,2048]{1,0:T(8,128)(2,1)} async-done(((bf16[256,1024]{1,0:T(8,128)(2,1)}), bf16[256,2048]{1,0:T(8,128)(2,1)}) %all-gather.7.cloned.1.call-update) | async-done | bytes 1048592 | tf_op jit(solution)/shard_map/all_gather | solution.py:38
  20.7 116.2 %all-gather.13.cloned.1.call-done = bf16[2,2048,1024]{2,1,0:T(8,128)(2,1)} async-done(((bf16[2,128,1024]{2,1,0:T(8,128)(2,1)}), bf16[2,2048,1024]{2,1,0:T(8,128)(2,1)}) %all-gather.13.cloned.1.call-update) | async-done | bytes 8388624 | tf_op jit(solution)/shard_map/all_gather | solution.py:32
  136.8 4.7 fusion.16
  141.5 108.4 %all-gather.11.cloned.1.call-done = bf16[2,2048,1024]{2,1,0:T(8,128)(2,1)} async-done(((bf16[2,128,1024]{2,1,0:T(8,128)(2,1)}), bf16[2,2048,1024]{2,1,0:T(8,128)(2,1)}) %all-gather.11.cloned.1.call-update) | async-done | bytes 8388624 | tf_op jit(solution)/shard_map/all_gather | solution.py:34
  250.0 3.8 fusion.14
  253.8 3.4 collective-permute-start
  257.2 135.4 %all-gather.15.cloned.1.call-done = bf16[2,1024,2048]{2,1,0:T(8,128)(2,1)} async-done(((bf16[2,1024,128]{2,1,0:T(8,128)(2,1)}), bf16[2,1024,2048]{2,1,0:T(8,128)(2,1)}) %all-gather.15.cloned.1.call-update) | async-done | bytes 8388624 | tf_op jit(solution)/shard_map/all_gather | solution.py:35
  392.6 113.0 %all-gather.9.cloned.1.call-done = bf16[2,2048,1024]{2,1,0:T(8,128)(2,1)} async-done(((bf16[2,128,1024]{2,1,0:T(8,128)(2,1)}), bf16[2,2048,1024]{2,1,0:T(8,128)(2,1)}) %all-gather.9.cloned.1.call-update) | async-done | bytes 8388624 | tf_op jit(solution)/shard_map/all_gather | solution.py:33
  505.6 7.0 %fusion.8 = bf16[256,2048]{1,0:T(8,128)(2,1)} fusion(bf16[2,1024,2048]{2,1,0:T(8,128)(2,1)} %all-gather.15.cloned.1.call-done, f32[2,1024]{1,0:T(2,128)S(1)} %collective-permute-done, f32[256,1024]{1,0:T(8,128)S(1)} %fusion.14, bf16[256,2048]{1,0:T(8,128)(2,1)S(1)} %copy-done.5, bf16[2,2048,1024]{2,1,0:T(8,128)(2,1)} %all-gather.9.cloned.1.call-done, ...), kind=kOutput, calls=%fused_computation.16 | convolution fusion | flops 2150891520 | bytes 11554816 | tf_op jit(solution)/shard_map/dot_general | solution.py:49
  512.7 0.0 all-gather.17.cloned.1.call-start
  512.8 6.6 %reduce-scatter.3.cloned.1.call-done = bf16[256,1024]{1,0:T(8,128)(2,1)} async-done(((bf16[256,2048]{1,0:T(8,128)(2,1)}), bf16[256,1024]{1,0:T(8,128)(2,1)}) %reduce-scatter.3.cloned.1.call-update) | async-done | bytes 524304 | tf_op jit(solution)/shard_map/reduce_scatter | solution.py:50
  519.4 1.4 fusion.38
  520.8 2.5 all-reduce.1
  523.3 2.2 add_convert_fusion.1
  525.5 0.0 reduce-scatter.5.cloned.1.call-start
  525.5 10.3 %all-gather.17.cloned.1.call-done = bf16[256,2048]{1,0:T(8,128)(2,1)} async-done(((bf16[256,1024]{1,0:T(8,128)(2,1)}), bf16[256,2048]{1,0:T(8,128)(2,1)}) %all-gather.17.cloned.1.call-update) | async-done | bytes 1048592 | tf_op jit(solution)/shard_map/all_gather | solution.py:38
  535.9 3.8 fusion.23
  539.7 3.5 fusion.21
  543.2 3.6 collective-permute-start.1
  546.9 1.3 collective-permute-done.1
  548.2 7.0 %fusion.9 = bf16[256,2048]{1,0:T(8,128)(2,1)} fusion(bf16[2,1024,2048]{2,1,0:T(8,128)(2,1)} %all-gather.15.cloned.1.call-done, f32[2,1024]{1,0:T(2,128)S(1)} %collective-permute-done.1, f32[256,1024]{1,0:T(8,128)S(1)} %fusion.21, bf16[256,2048]{1,0:T(8,128)(2,1)S(1)} %copy-done.6, bf16[2,2048,1024]{2,1,0:T(8,128)(2,1)} %all-gather.9.cloned.1.call-done, ...), kind=kOutput, calls=%fused_computation.17 | convolution fusion | flops 2150891520 | bytes 11554816 | tf_op jit(solution)/shard_map/dot_general | solution.py:49
  555.3 10.3 %reduce-scatter.5.cloned.1.call-done = bf16[256,1024]{1,0:T(8,128)(2,1)} async-done(((bf16[256,2048]{1,0:T(8,128)(2,1)}), bf16[256,1024]{1,0:T(8,128)(2,1)}) %reduce-scatter.5.cloned.1.call-update) | async-done | bytes 524304 | tf_op jit(solution)/shard_map/reduce_scatter | solution.py:50
  565.5 1.4 fusion.39
  566.9 2.5 all-reduce
  569.4 2.2 add_convert_fusion
  (29 shorter events, 0.3 us)
Async XLA Ops:
  6.5 14.1 %all-gather.7.cloned.1.call-start = ((), (), s32[]{:S(2)}) async-start(), calls=%async_computation.2 | async-start | bytes 1572864 | tf_op jit(solution)/shard_map/all_gather | solution.py:38
  7.3 129.6 %all-gather.13.cloned.1.call-start = ((), (), s32[]{:S(2)}) async-start(), calls=%async_computation.5 | async-start | bytes 8912896 | tf_op jit(solution)/shard_map/all_gather | solution.py:32
  8.0 242.0 %all-gather.11.cloned.1.call-start = ((), (), s32[]{:S(2)}) async-start(), calls=%async_computation.4 | async-start | bytes 8912896 | tf_op jit(solution)/shard_map/all_gather | solution.py:34
  8.7 383.9 %all-gather.15.cloned.1.call-start = ((), (), s32[]{:S(2)}) async-start(), calls=%async_computation.6 | async-start | bytes 8912896 | tf_op jit(solution)/shard_map/all_gather | solution.py:35
  9.3 496.3 %all-gather.9.cloned.1.call-start = ((), (), s32[]{:S(2)}) async-start(), calls=%async_computation.3 | async-start | bytes 8912896 | tf_op jit(solution)/shard_map/all_gather | solution.py:33
  9.9 247.2 %copy-start.2 = (f32[2,3,1024]{2,0,1:T(2,128)S(1)}, f32[2,3,1024]{2,0,1:T(2,128)}, u32[]{:S(2)}) copy-start(f32[2,3,1024]{2,0,1:T(2,128)} %param.12) | copy-start | bytes 73732
  9.9 509.5 %reduce-scatter.3.cloned.1.call-start = ((), (), s32[]{:S(2)}) async-start(), calls=%async_computation.7 | async-start | bytes 1572864 | tf_op jit(solution)/shard_map/reduce_scatter | solution.py:50
  20.7 229.3 %copy-start.5 = (bf16[256,2048]{1,0:T(8,128)(2,1)S(1)}, bf16[256,2048]{1,0:T(8,128)(2,1)}, u32[]{:S(2)}) copy-start(bf16[256,2048]{1,0:T(8,128)(2,1)} %all-gather.7.cloned.1.call-done) | copy-start | bytes 3145732
  253.8 251.9 %collective-permute-start = (f32[2,1024]{1,0:T(2,128)S(1)}, f32[2,1024]{1,0:T(2,128)S(1)}, u32[]{:S(2)}, u32[]{:S(2)}) collective-permute-start(f32[2,1024]{1,0:T(2,128)S(1)} %slice.99), channel_id=1, source_target_pairs={{0,2},{2,4},{4,6},{6,8},{8,10},{10,12},{12,14},{14,16},{16,18},{18... | collective-permute-start | bytes 24584 | tf_op jit(solution)/shard_map/ppermute | solution.py:13
  505.6 7.1 %copy-start.3 = (f32[2,1024]{1,0:T(2,128)S(1)}, f32[2,1024]{1,0:T(2,128)}, u32[]{:S(2)}) copy-start(f32[2,1024]{1,0:T(2,128)} %param.14) | copy-start | bytes 24580
  505.6 7.2 %copy-start.4 = (f32[2,1024]{1,0:T(2,128)S(1)}, f32[2,1024]{1,0:T(2,128)}, u32[]{:S(2)}) copy-start(f32[2,1024]{1,0:T(2,128)} %param.15) | copy-start | bytes 24580
  505.6 13.8 %copy-start.1 = (bf16[256,1024]{1,0:T(8,128)(2,1)S(1)}, bf16[256,1024]{1,0:T(8,128)(2,1)}, u32[]{:S(2)}) copy-start(bf16[256,1024]{1,0:T(8,128)(2,1)} %param.8) | copy-start | bytes 1572868
  512.7 23.1 %all-gather.17.cloned.1.call-start = ((), (), s32[]{:S(2)}) async-start(), calls=%async_computation.8 | async-start | bytes 1572864 | tf_op jit(solution)/shard_map/all_gather | solution.py:38
  525.5 40.1 %reduce-scatter.5.cloned.1.call-start = ((), (), s32[]{:S(2)}) async-start(), calls=%async_computation.9 | async-start | bytes 1572864 | tf_op jit(solution)/shard_map/reduce_scatter | solution.py:50
  535.9 3.8 copy-start.6
  543.2 5.0 collective-permute-start.1
  548.2 17.3 %copy-start = (bf16[256,1024]{1,0:T(8,128)(2,1)S(1)}, bf16[256,1024]{1,0:T(8,128)(2,1)}, u32[]{:S(2)}) copy-start(bf16[256,1024]{1,0:T(8,128)(2,1)} %add_convert_fusion.1) | copy-start | bytes 1572868
Sparse Core Ops, SparseCore 0:
  8.9 11.7 all-gather.6
  23.4 113.3 all-gather.12
  139.6 110.3 all-gather.10
  252.6 140.0 all-gather.14
  395.2 110.3 all-gather.8
  512.8 6.5 reduce-scatter.2
  525.6 10.2 all-gather.16
  555.4 10.0 reduce-scatter.4
where the time goes:
time: 579 us; the launch traced here: 578 us
  waiting for transfers between devices  515 us (89%)
  matrix products  29.9 us (5%)
  between operations  13.6 us (2%)
  starting transfers between devices  7.27 us (1%)
  other arithmetic  7.1 us (1%)
    all_gather x1, waiting for transfers between devices, shards(): lax.all_gather(output_weight, 'sp', axis=2, tiled=True)  135 us
    all_gather x1, waiting for transfers between devices, shards(): lax.all_gather(value_weight, 'sp', axis=1, tiled=True)  116 us
    all_gather x1, waiting for transfers between devices, shards(): lax.all_gather(outer_weight, 'sp', axis=1, tiled=True)  113 us
    all_gather x1, waiting for transfers between devices, shards(): lax.all_gather(inner_weight, 'sp', axis=1, tiled=True)  108 us
    all_gather x2, waiting for transfers between devices, shards(): whole = lax.all_gather(state, 'tp', axis=1, tiled=True)  21 us
    reduce_scatter x2, waiting for transfers between devices, shards(): lax.psum_scatter(terms.astype(jnp.bfloat16), 'tp', scatter_dimension=1, t...  16.9 us
    dot_general x4, matrix products, input_products(): jnp.dot(whole, weight, preferred_element_type=jnp.float32)  15.8 us
    dot_general x2, matrix products, shards(): jnp.dot(gated, all_output[layer], preferred_element_type=jnp.float32)  14.1 us
  transfers between devices with their start and end apart: 10, of which 9 were waited for; matrix products, arithmetic and copies ran while one was open for 1% of the time, Pallas kernels for 0%

commit v1 on v0

--- a/solution.py
+++ b/solution.py
@@ -5,6 +5,11 @@
 
 D = 2048
 LAYERS = 2
+
+
+def stack_and_merge(x, name, along):
+    parts = lax.all_gather(x, name)
+    return jnp.concatenate(parts, axis=along)
 
 
 def from_behind(array, axis, by):
@@ -29,7 +34,7 @@
     state = tokens
     taps_count = conv_taps.shape[1]
     all_value, all_outer, all_inner, all_output = (
-        lax.all_gather(value_weight, "sp", axis=1, tiled=True),
+        stack_and_merge(value_weight, "sp", 1),
         lax.all_gather(outer_weight, "sp", axis=1, tiled=True),
         lax.all_gather(inner_weight, "sp", axis=1, tiled=True),
         lax.all_gather(output_weight, "sp", axis=2, tiled=True),

time: 579 us -> 579 us (level)
  local copies, waits for them, and re-layouts: 0.08 us -> 6.27 us
  waiting for transfers between devices: 515 us -> 509 us
    all_gather x2, waiting for transfers between devices: 21 us -> 12.9 us  [shards(): whole = lax.all_gather(state, 'tp', axis=1, tiled=True)]
    all_gather x1, waiting for transfers between devices: 135 us -> 143 us  [shards(): lax.all_gather(output_weight, 'sp', axis=2, tiled=True)]
    all_gather x1, waiting for transfers between devices: 113 us -> 106 us  [shards(): lax.all_gather(outer_weight, 'sp', axis=1, tiled=True)]
    slice x0 -> x1, local copies, waits for them, and re-layouts: none -> 6.19 us  [shards(): all_value[layer]]
  transfers between devices with their start and end apart: 10 -> 10, of which waited for: 9 -> 9; matrix products, arithmetic and copies ran while one was open for 1% -> 3% of each run, Pallas kernels for 0% -> 0%
where the time goes in v1:
time: 579 us
  waiting for transfers between devices  509 us (88%)
  matrix products  30.2 us (5%)
  between operations  13.6 us (2%)
  starting transfers between devices  7.27 us (1%)
  other arithmetic  7.09 us (1%)
  local copies, waits for them, and re-layouts  6.27 us (1%)
    all_gather x1, waiting for transfers between devices, shards(): lax.all_gather(output_weight, 'sp', axis=2, tiled=True)  143 us
    all_gather x1, waiting for transfers between devices, stack_and_merge(): parts = lax.all_gather(x, name)  115 us
    all_gather x1, waiting for transfers between devices, shards(): lax.all_gather(inner_weight, 'sp', axis=1, tiled=True)  111 us
    all_gather x1, waiting for transfers between devices, shards(): lax.all_gather(outer_weight, 'sp', axis=1, tiled=True)  106 us
    reduce_scatter x2, waiting for transfers between devices, shards(): lax.psum_scatter(terms.astype(jnp.bfloat16), 'tp', scatter_dimension=1, t...  16.9 us
    dot_general x4, matrix products, input_products(): jnp.dot(whole, weight, preferred_element_type=jnp.float32)  16 us
    dot_general x2, matrix products, shards(): jnp.dot(gated, all_output[layer], preferred_element_type=jnp.float32)  14.1 us
    all_gather x2, waiting for transfers between devices, shards(): whole = lax.all_gather(state, 'tp', axis=1, tiled=True)  12.9 us
  transfers between devices with their start and end apart: 10, of which 9 were waited for; matrix products, arithmetic and copies ran while one was open for 3% of the time, Pallas kernels for 0%

profile of v1, /device:TPU:0, one launch (start us, length us, event | category | flops | bytes accessed | tf_op | source)
XLA Modules:
  0.0 578.6 jit_solution(6971229221123413728)
XLA Ops:
  6.5 0.7 all-gather.18.cloned.1.call-update
  7.3 0.7 all-gather.8.cloned.1.call-update
  8.1 0.7 all-gather.12.cloned.1.call-update
  8.8 0.5 all-gather.10.cloned.1.call-update
  9.4 0.5 all-gather.14.cloned.1.call-update
  9.9 0.0 reduce-scatter.3.cloned.1.call-start
  10.0 115.2 %all-gather.18.cloned.1.call-done = bf16[32,128,1024]{2,1,0:T(8,128)(2,1)} async-done(((bf16[2,128,1024]{2,1,0:T(8,128)(2,1)}), bf16[32,128,1024]{2,1,0:T(8,128)(2,1)}) %all-gather.18.cloned.1.call-update) | async-done | bytes 8388624 | tf_op jit(solution)/shard_map/all_gather | solution.py:11
  125.2 6.2 %fusion.46 = (bf16[1,16,128,1024]{3,2,0,1:T(8,128)(2,1)}, bf16[1,16,128,1024]{3,2,0,1:T(8,128)(2,1)}) fusion(bf16[2,16,128,1024]{3,2,0,1:T(8,128)(2,1)} %bitcast.81), kind=kLoop, calls=%fused_computation.68 | loop fusion | bytes 16777216 | tf_op jit(solution)/shard_map/slice | solution.py:45
  131.4 2.6 all-gather.8.cloned.1.call-done
  133.9 4.9 fusion.19
  138.8 111.3 %all-gather.12.cloned.1.call-done = bf16[2,2048,1024]{2,1,0:T(8,128)(2,1)} async-done(((bf16[2,128,1024]{2,1,0:T(8,128)(2,1)}), bf16[2,2048,1024]{2,1,0:T(8,128)(2,1)}) %all-gather.12.cloned.1.call-update) | async-done | bytes 8388624 | tf_op jit(solution)/shard_map/all_gather | solution.py:39
  250.1 3.8 fusion.12
  253.9 3.4 collective-permute-start
  257.3 105.8 %all-gather.10.cloned.1.call-done = bf16[2,2048,1024]{2,1,0:T(8,128)(2,1)} async-done(((bf16[2,128,1024]{2,1,0:T(8,128)(2,1)}), bf16[2,2048,1024]{2,1,0:T(8,128)(2,1)}) %all-gather.10.cloned.1.call-update) | async-done | bytes 8388624 | tf_op jit(solution)/shard_map/all_gather | solution.py:38
  363.1 142.6 %all-gather.14.cloned.1.call-done = bf16[2,1024,2048]{2,1,0:T(8,128)(2,1)} async-done(((bf16[2,1024,128]{2,1,0:T(8,128)(2,1)}), bf16[2,1024,2048]{2,1,0:T(8,128)(2,1)}) %all-gather.14.cloned.1.call-update) | async-done | bytes 8388624 | tf_op jit(solution)/shard_map/all_gather | solution.py:40
  505.7 7.1 %fusion.6 = bf16[256,2048]{1,0:T(8,128)(2,1)} fusion(bf16[2,1024,2048]{2,1,0:T(8,128)(2,1)} %all-gather.14.cloned.1.call-done, f32[2,1024]{1,0:T(2,128)S(1)} %collective-permute-done, f32[256,1024]{1,0:T(8,128)S(1)} %fusion.12, bf16[256,2048]{1,0:T(8,128)(2,1)S(1)} %copy-done.5, bf16[2,2048,1024]{2,1,0:T(8,128)(2,1)} %all-gather.10.cloned.1.call-done, ...), kind=kOutput, calls=%fused_computation.12 | convolution fusion | flops 2150891520 | bytes 11554816 | tf_op jit(solution)/shard_map/dot_general | solution.py:54
  512.9 0.0 all-gather.16.cloned.1.call-start
  513.0 6.6 %reduce-scatter.3.cloned.1.call-done = bf16[256,1024]{1,0:T(8,128)(2,1)} async-done(((bf16[256,2048]{1,0:T(8,128)(2,1)}), bf16[256,1024]{1,0:T(8,128)(2,1)}) %reduce-scatter.3.cloned.1.call-update) | async-done | bytes 524304 | tf_op jit(solution)/shard_map/reduce_scatter | solution.py:55
  519.6 1.4 fusion.34
  521.0 2.5 all-reduce.1
  523.5 2.1 add_convert_fusion.1
  525.7 0.0 reduce-scatter.5.cloned.1.call-start
  525.7 10.3 %all-gather.16.cloned.1.call-done = bf16[256,2048]{1,0:T(8,128)(2,1)} async-done(((bf16[256,1024]{1,0:T(8,128)(2,1)}), bf16[256,2048]{1,0:T(8,128)(2,1)}) %all-gather.16.cloned.1.call-update) | async-done | bytes 1048592 | tf_op jit(solution)/shard_map/all_gather | solution.py:43
  536.0 3.9 fusion.18
  539.9 3.5 fusion.17
  543.4 3.6 collective-permute-start.1
  547.0 1.3 collective-permute-done.1
  548.4 7.0 %fusion.7 = bf16[256,2048]{1,0:T(8,128)(2,1)} fusion(bf16[2,1024,2048]{2,1,0:T(8,128)(2,1)} %all-gather.14.cloned.1.call-done, f32[2,1024]{1,0:T(2,128)S(1)} %collective-permute-done.1, f32[256,1024]{1,0:T(8,128)S(1)} %fusion.17, bf16[256,2048]{1,0:T(8,128)(2,1)S(1)} %copy-done.6, bf16[2,2048,1024]{2,1,0:T(8,128)(2,1)} %all-gather.10.cloned.1.call-done, ...), kind=kOutput, calls=%fused_computation.13 | convolution fusion | flops 2150891520 | bytes 11554816 | tf_op jit(solution)/shard_map/dot_general | solution.py:54
  555.4 10.3 %reduce-scatter.5.cloned.1.call-done = bf16[256,1024]{1,0:T(8,128)(2,1)} async-done(((bf16[256,2048]{1,0:T(8,128)(2,1)}), bf16[256,1024]{1,0:T(8,128)(2,1)}) %reduce-scatter.5.cloned.1.call-update) | async-done | bytes 524304 | tf_op jit(solution)/shard_map/reduce_scatter | solution.py:55
  565.7 1.4 fusion.35
  567.1 2.5 all-reduce
  569.6 2.1 add_convert_fusion
  (30 shorter events, 0.3 us)
Async XLA Ops:
  6.5 118.6 %all-gather.18.cloned.1.call-start = ((), (), s32[]{:S(2)}) async-start(), calls=%async_computation.9 | async-start | bytes 8912896 | tf_op jit(solution)/shard_map/all_gather | solution.py:11
  7.3 126.7 %all-gather.8.cloned.1.call-start = ((), (), s32[]{:S(2)}) async-start(), calls=%async_computation.2 | async-start | bytes 1572864 | tf_op jit(solution)/shard_map/all_gather | solution.py:43
  8.0 242.1 %all-gather.12.cloned.1.call-start = ((), (), s32[]{:S(2)}) async-start(), calls=%async_computation.4 | async-start | bytes 8912896 | tf_op jit(solution)/shard_map/all_gather | solution.py:39
  8.7 354.4 %all-gather.10.cloned.1.call-start = ((), (), s32[]{:S(2)}) async-start(), calls=%async_computation.3 | async-start | bytes 8912896 | tf_op jit(solution)/shard_map/all_gather | solution.py:38
  9.3 496.4 %all-gather.14.cloned.1.call-start = ((), (), s32[]{:S(2)}) async-start(), calls=%async_computation.5 | async-start | bytes 8912896 | tf_op jit(solution)/shard_map/all_gather | solution.py:40
  9.9 509.7 %reduce-scatter.3.cloned.1.call-start = ((), (), s32[]{:S(2)}) async-start(), calls=%async_computation.6 | async-start | bytes 1572864 | tf_op jit(solution)/shard_map/reduce_scatter | solution.py:55
  133.9 116.2 %copy-start.5 = (bf16[256,2048]{1,0:T(8,128)(2,1)S(1)}, bf16[256,2048]{1,0:T(8,128)(2,1)}, u32[]{:S(2)}) copy-start(bf16[256,2048]{1,0:T(8,128)(2,1)} %all-gather.8.cloned.1.call-done) | copy-start | bytes 3145732
  138.8 118.4 %copy-start.2 = (f32[2,3,1024]{2,0,1:T(2,128)S(1)}, f32[2,3,1024]{2,0,1:T(2,128)}, u32[]{:S(2)}) copy-start(f32[2,3,1024]{2,0,1:T(2,128)} %param.12) | copy-start | bytes 73732
  253.9 251.9 %collective-permute-start = (f32[2,1024]{1,0:T(2,128)S(1)}, f32[2,1024]{1,0:T(2,128)S(1)}, u32[]{:S(2)}, u32[]{:S(2)}) collective-permute-start(f32[2,1024]{1,0:T(2,128)S(1)} %slice.101), channel_id=1, source_target_pairs={{0,2},{2,4},{4,6},{6,8},{8,10},{10,12},{12,14},{14,16},{16,18},{18... | collective-permute-start | bytes 24584 | tf_op jit(solution)/shard_map/ppermute | solution.py:18
  505.7 7.2 %copy-start.3 = (f32[2,1024]{1,0:T(2,128)S(1)}, f32[2,1024]{1,0:T(2,128)}, u32[]{:S(2)}) copy-start(f32[2,1024]{1,0:T(2,128)} %param.14) | copy-start | bytes 24580
  505.7 7.2 %copy-start.4 = (f32[2,1024]{1,0:T(2,128)S(1)}, f32[2,1024]{1,0:T(2,128)}, u32[]{:S(2)}) copy-start(f32[2,1024]{1,0:T(2,128)} %param.15) | copy-start | bytes 24580
  505.7 13.9 %copy-start.1 = (bf16[256,1024]{1,0:T(8,128)(2,1)S(1)}, bf16[256,1024]{1,0:T(8,128)(2,1)}, u32[]{:S(2)}) copy-start(bf16[256,1024]{1,0:T(8,128)(2,1)} %param.8) | copy-start | bytes 1572868
  512.9 23.1 %all-gather.16.cloned.1.call-start = ((), (), s32[]{:S(2)}) async-start(), calls=%async_computation.7 | async-start | bytes 1572864 | tf_op jit(solution)/shard_map/all_gather | solution.py:43
  525.7 40.1 %reduce-scatter.5.cloned.1.call-start = ((), (), s32[]{:S(2)}) async-start(), calls=%async_computation.8 | async-start | bytes 1572864 | tf_op jit(solution)/shard_map/reduce_scatter | solution.py:55
  536.0 3.9 copy-start.6
  543.4 5.0 collective-permute-start.1
  548.4 17.3 %copy-start = (bf16[256,1024]{1,0:T(8,128)(2,1)S(1)}, bf16[256,1024]{1,0:T(8,128)(2,1)}, u32[]{:S(2)}) copy-start(bf16[256,1024]{1,0:T(8,128)(2,1)} %add_convert_fusion.1) | copy-start | bytes 1572868
Sparse Core Ops, SparseCore 0:
  10.1 115.0 all-gather.17
  126.7 7.1 all-gather.7
  136.7 113.3 all-gather.11
  252.7 110.3 all-gather.9
  365.7 140.0 all-gather.13
  513.0 6.5 reduce-scatter.2
  525.8 10.1 all-gather.15
  555.6 10.0 reduce-scatter.4
